TPU v7x, 32 devices: a whole 2x2x4 slice. The times are simulated.
32 devices in a mesh: sp: 16 (over z, y, x), tp: 2 (over core).
Axes of the slice: x: 2, y: 2, z: 4, core: 2. Of those that a mesh axis runs over, the one named last changes fastest.
Arguments:
- queries_small: bfloat16 [4096, 1024], P('sp', 'tp'), may hold values from -160 to 160
- queries_large: bfloat16 [4096, 1024], P('sp', 'tp'), may hold values from -160 to 160
- kv_small: bfloat16 [4096, 128], P('sp'), may hold values from -4 to 4
- kv_large: bfloat16 [4096, 256], P('sp'), may hold values from -4 to 4
- cum_small: float32 [16, 4096], P('tp', 'sp'), may hold values from -514 to 0, as said below
- cum_large: float32 [8, 4096], P('tp', 'sp'), may hold values from -514 to 0, as said below
- residual: bfloat16 [4096, 2048], P(('sp', 'tp')), may hold values from -6 to 6
- out_small: bfloat16 [1024, 2048], replicated, may hold values from -0.125 to 0.125
- out_large: bfloat16 [1024, 2048], replicated, may hold values from -0.125 to 0.125
- gain_mix: float32 [2048], replicated, may hold values from 0.1 to 1.9
- gain_route: float32 [2048], replicated, may hold values from 0.1 to 1.9
- gain_blend: float32 [2048], replicated, may hold values from 0.1 to 1.9
- w_gate: bfloat16 [32, 2048, 1024], P(('sp', 'tp')), may hold values from -0.125 to 0.125
- w_up: bfloat16 [32, 2048, 1024], P(('sp', 'tp')), may hold values from -0.125 to 0.125
- w_down: bfloat16 [32, 1024, 2048], P(('sp', 'tp')), may hold values from -0.1875 to 0.1875
- route: int32 [2, 4096], P(None, ('sp', 'tp')), may hold values from 0 to 31, as said below
- route_bias: float32 [4096], P(('sp', 'tp')), may hold values from -6 to 6
Outputs:
- result: bfloat16 [4096, 2048], P(('sp', 'tp'))
Inputs may be any that keep to these rules, and one draw needn't show every extreme that they name: `cum_small`: each row is non-increasing along positions. `cum_large`: each row is non-increasing along positions. route[0, t] and route[1, t] are different experts of the same group of 8 consecutive experts. Among the 128 positions of one device (aligned blocks), no expert is named by more than 16 of them; in every draw all experts of one group are named by exactly 16 positions of every device. Within one device's positions the loads of the experts of one group differ by at most 2.
All inputs are finite; a program needn't handle non-finite values.
Results may differ from a plain program's by a relative error of at most 0.014.
Values may be sent and summed in bfloat16 or wider, within the bound.
A program may use at most 128 MiB of HBM per device.

v0:
```python
import math
import jax
import jax.numpy as jnp
from jax import lax
from jax.sharding import PartitionSpec as P

norm_eps = 1e-06
far_score = -1e30


def rms_scale(values, gain_row):
    return (
        values * lax.rsqrt(jnp.mean(values * values, axis=-1, keepdims=True) + norm_eps) * gain_row
    )


def online_update(carried, queries, query_cum, keys_values, key_cum, key_pos, query_pos):
    running_max, running_sum, weighted = carried
    head_size = keys_values.shape[1] // 2
    key_rows = keys_values[:, :head_size]
    value_rows = keys_values[:, head_size:]
    scores = jnp.einsum(
        "qhd,kd->hqk", queries, key_rows, preferred_element_type=jnp.float32
    ) * head_size ** (-0.5)
    scores = scores + query_cum[:, :, None] - key_cum[:, None, :]
    allowed = key_pos[None, None, :] <= query_pos[None, :, None]
    scores = jnp.where(allowed, scores, far_score)
    newest = jnp.maximum(running_max, jnp.max(scores, axis=-1))
    weights = jnp.where(allowed, jnp.exp(scores - newest[:, :, None]), 0.0)
    factor = jnp.exp(running_max - newest)
    running_sum = running_sum * factor + jnp.sum(weights, axis=-1)
    weighted = weighted * factor[:, :, None] + jnp.einsum(
        "hqk,kd->hqd", weights.astype(jnp.bfloat16), value_rows, preferred_element_type=jnp.float32
    )
    return (newest, running_sum, weighted)


def attend_keys(
    softmax_state,
    query_small,
    query_large,
    qcum_small,
    qcum_large,
    query_pos,
    part_small,
    part_large,
    key_pos,
    kcum_small,
    kcum_large,
):
    key_count = key_pos.shape[0]
    block_width = math.gcd(key_count, 2048)
    blocks = key_count // block_width
    pieces = (
        part_small.reshape(blocks, block_width, part_small.shape[1]),
        part_large.reshape(blocks, block_width, part_large.shape[1]),
        key_pos.reshape(blocks, block_width),
        kcum_small.reshape(kcum_small.shape[0], blocks, block_width).transpose(1, 0, 2),
        kcum_large.reshape(kcum_large.shape[0], blocks, block_width).transpose(1, 0, 2),
    )
    query_last = query_pos[-1]

    def advance(carried, block_data):
        kv_one, kv_two, positions, cum_one, cum_two = block_data

        def compute(current):
            return (
                online_update(
                    current[0], query_small, qcum_small, kv_one, cum_one, positions, query_pos
                ),
                online_update(
                    current[1], query_large, qcum_large, kv_two, cum_two, positions, query_pos
                ),
            )

        return (
            lax.cond(jnp.min(positions) <= query_last, compute, lambda current: current, carried),
            None,
        )

    softmax_state, _ = lax.scan(advance, softmax_state, pieces)
    return softmax_state


def finish(carried):
    running_max, running_sum, weighted = carried
    outputs = (weighted / running_sum[:, :, None]).astype(jnp.bfloat16)
    return outputs.transpose(1, 0, 2).reshape(outputs.shape[1], outputs.shape[0] * outputs.shape[2])


def fresh_state(head_count, query_count, head_size):
    return (
        jnp.full((head_count, query_count), far_score, jnp.float32),
        jnp.zeros((head_count, query_count), jnp.float32),
        jnp.zeros((head_count, query_count, head_size), jnp.float32),
    )


def on_device(
    queries_small,
    queries_large,
    kv_small,
    kv_large,
    cum_small,
    cum_large,
    residual,
    out_small,
    out_large,
    gain_mix,
    gain_route,
    gain_blend,
    w_gate,
    w_up,
    w_down,
    route,
    route_bias,
):
    tokens_here = queries_small.shape[0]
    heads_small = cum_small.shape[0]
    heads_large = cum_large.shape[0]
    size_small = kv_small.shape[1] // 2
    size_large = kv_large.shape[1] // 2
    query_small = queries_small.reshape(tokens_here, heads_small, size_small)
    query_large = queries_large.reshape(tokens_here, heads_large, size_large)
    query_pos = lax.axis_index("sp") * tokens_here + jnp.arange(tokens_here, dtype=jnp.int32)
    cum_all = (
        lax.all_gather(cum_small, "sp", axis=1, tiled=True),
        lax.all_gather(cum_large, "sp", axis=1, tiled=True),
    )
    start_state = (
        fresh_state(heads_small, tokens_here, size_small),
        fresh_state(heads_large, tokens_here, size_large),
    )
    block_data = (
        lax.all_gather(kv_small, "sp", axis=0, tiled=True),
        lax.all_gather(kv_large, "sp", axis=0, tiled=True),
    )
    key_count = block_data[0].shape[0]
    key_pos = jnp.arange(key_count, dtype=jnp.int32)
    kcum_small = cum_all[0]
    kcum_large = cum_all[1]
    softmax_state = attend_keys(
        start_state,
        query_small,
        query_large,
        cum_small,
        cum_large,
        query_pos,
        block_data[0],
        block_data[1],
        key_pos,
        kcum_small,
        kcum_large,
    )
    attn_small = finish(softmax_state[0])
    attn_large = finish(softmax_state[1])
    row_count = tokens_here // lax.axis_size("tp")
    whole_small, whole_large = (
        lax.all_to_all(attn_small, "tp", split_axis=0, concat_axis=1, tiled=True),
        lax.all_to_all(attn_large, "tp", split_axis=0, concat_axis=1, tiled=True),
    )
    mixer_out = jnp.dot(whole_small, out_small, preferred_element_type=jnp.float32) + jnp.dot(
        whole_large, out_large, preferred_element_type=jnp.float32
    )
    mixed = (residual.astype(jnp.float32) + rms_scale(mixer_out, gain_mix)).astype(jnp.bfloat16)
    routed = rms_scale(mixed.astype(jnp.float32), gain_route).astype(jnp.bfloat16)
    experts = lax.axis_size(("sp", "tp"))
    capacity = 4 * row_count // experts
    flat_ids = route.reshape(2 * row_count)
    marked = (flat_ids[:, None] == jnp.arange(experts, dtype=jnp.int32)[None, :]).astype(jnp.int32)
    ranked = jnp.sum((jnp.cumsum(marked, axis=0) - 1) * marked, axis=1)
    slot_ids = flat_ids * capacity + ranked
    dispatch_table = (
        slot_ids[:, None] == jnp.arange(experts * capacity, dtype=jnp.int32)[None, :]
    ).astype(jnp.bfloat16)
    dispatch_table = dispatch_table[:row_count] + dispatch_table[row_count:]
    outgoing = jnp.einsum(
        "rs,rd->sd", dispatch_table, routed, preferred_element_type=jnp.float32
    ).astype(jnp.bfloat16)
    outgoing = outgoing.reshape(experts, capacity, routed.shape[1])
    received = lax.all_to_all(outgoing, ("sp", "tp"), split_axis=0, concat_axis=0, tiled=True)
    row_total = received.shape[0] * received.shape[1]
    expert_rows = received.reshape(row_total, received.shape[2])
    gate_pre = jnp.dot(expert_rows, w_gate[0], preferred_element_type=jnp.float32)
    up_pre = jnp.dot(expert_rows, w_up[0], preferred_element_type=jnp.float32)
    hidden = (jax.nn.silu(gate_pre) * up_pre).astype(jnp.bfloat16)
    expert_out = jnp.dot(hidden, w_down[0], preferred_element_type=jnp.float32).astype(jnp.bfloat16)
    returned = lax.all_to_all(
        expert_out.reshape(received.shape), ("sp", "tp"), split_axis=0, concat_axis=0, tiled=True
    )
    picked = returned.reshape(experts * capacity, routed.shape[1])[slot_ids].astype(jnp.float32)
    blended = (
        jax.nn.sigmoid(route_bias)[:, None] * picked[:row_count]
        + jax.nn.sigmoid(-route_bias)[:, None] * picked[row_count:]
    )
    return (mixed.astype(jnp.float32) + rms_scale(blended, gain_blend)).astype(jnp.bfloat16)


def solution(mesh):
    in_specs = (
        P("sp", "tp"),
        P("sp", "tp"),
        P("sp", None),
        P("sp", None),
        P("tp", "sp"),
        P("tp", "sp"),
        P(("sp", "tp"), None),
        P(),
        P(),
        P(),
        P(),
        P(),
        P(("sp", "tp"), None, None),
        P(("sp", "tp"), None, None),
        P(("sp", "tp"), None, None),
        P(None, ("sp", "tp")),
        P(("sp", "tp")),
    )
    out_specs = P(("sp", "tp"), None)
    return jax.shard_map(
        on_device, mesh=mesh, in_specs=in_specs, out_specs=out_specs, check_vma=False
    )
```

profile of v0, /device:TPU:0, one launch (start us, length us, event | category | flops | bytes accessed | tf_op | source)
XLA Modules:
  0.0 335.0 jit_solution(12341823653482546608)
XLA Ops:
  8.7 1.1 copy.42
  9.8 1.1 copy.43
  12.5 43.1 %all_gather.15 = f32[4,4096]{1,0:T(4,128)S(1)} all-gather(f32[4,256]{1,0:T(4,128)} %param.26), channel_id=1, replica_groups=mesh['sp'=16,'tp'=2] {'sp'}, dimensions={1}, use_global_device_ids=true | all-gather | bytes 69632 | tf_op jit(solution)/shard_map/all_gather | solution.py:128
  55.7 36.7 %all_gather.13 = f32[8,4096]{1,0:T(8,128)S(1)} all-gather(f32[8,256]{1,0:T(8,128)} %param.25), channel_id=1, replica_groups=mesh['sp'=16,'tp'=2] {'sp'}, dimensions={1}, use_global_device_ids=true | all-gather | bytes 139264 | tf_op jit(solution)/shard_map/all_gather | solution.py:127
  92.4 0.8 fusion.58
  93.8 0.8 fusion.53
  94.7 1.5 copy.44
  96.2 34.1 %all-gather.5.cloned.1.call-done = bf16[4096,256]{1,0:T(8,128)(2,1)} async-done(((bf16[256,256]{1,0:T(8,128)(2,1)}), bf16[4096,256]{1,0:T(8,128)(2,1)}) %all-gather.5.cloned.1.call-update) | async-done | bytes 2097168 | tf_op jit(solution)/shard_map/all_gather | solution.py:136
  130.4 30.6 %while.21 = (s32[]{:T(128)}, f32[8,256]{1,0:T(8,128)S(1)}, f32[8,256]{1,0:T(8,128)S(1)}, f32[8,256,64]{1,2,0:T(8,128)S(1)}, f32[4,256]{1,0:T(4,128)S(1)}, /*inde...) while((s32[]{:T(128)}, f32[8,256]{1,0:T(8,128)S(1)}, ...), condition=%wide.region_8.9_spmd.clone, body=%wide.region_0.8_spmd.clone.sunk | while | flops 2268078336 | bytes 95699496 | solution.py:81
  130.4 0.7 fusion.72
  132.4 26.2 %conditional.3 = ((f32[8,256]{1,0:T(8,128)S(1)}, f32[8,256]{1,0:T(8,128)S(1)}, f32[8,256,64]{1,2,0:T(8,128)S(1)}, f32[4,256]{1,0:T(4,128)S(1)}, f32[4,256]{1,0:T(4,128)S(1)}, /*index=5*/f32[4,256,128]{2,1,0:T(8,128)S(1)})) conditional(s32[]{:T(128)} %convert_element_type.110, (f32[8,256]{1,0:T(8,128)S(1)}, f32[8,256]{1,0:T(8,128)S(1)}, ...), branch_computations={%region_2.2_spmd, %region_3.7_spmd} | conditional | flops 2268076288 | bytes 95681696 | solution.py:77
  133.0 5.0 %fusion.6 = (f32[8,256]{1,0:T(8,128)S(1)}, f32[2048,256,8]{1,0,2:T(8,128)S(1)}) fusion(f32[8,2048]{1,0:T(8,128)S(1)} %dynamic-slice_bitcast_fusion.2, f32[8,256]{1,0:T(8,128)} %get-tuple-element.221, pred[256,2048]{0,1:T(8,128)(4,1)S(1)} %broadcast_compare_fusion, bf16[256,8,64]{0,2,1:T(8,128)(2,1)S(1)} %get-tuple-element.220, ...), kind=kOutput, calls=%fused_computation.8 | convolution fusion | flops 557840384 | bytes 17907712 | tf_op jit(solution)/shard_map/while/body/eval_jaxpr/cond/branch_1_fun/qhd,kd->hqk/dot_general | solution.py:22
  138.1 6.0 %fusion.5 = f32[8,256]{1,0:T(8,128)S(1)} fusion(f32[2048,256,8]{1,0,2:T(8,128)S(1)} %get-tuple-element.412, f32[8,256]{1,0:T(8,128)S(1)} %max.8, f32[8,2048]{1,0:T(8,128)S(1)} %dynamic-slice_bitcast_fusion.2, f32[8,256]{1,0:T(8,128)S(1)} %copy-done.3, pred[256,2048]{0,1:T(8,128)(4,1)S(1)} %broadcast_compare_fusion), kind=kLoop, calls=%fused_computation.7 | loop fusion | flops 29358080 | bytes 17391616 | tf_op jit(solution)/shard_map/while/body/eval_jaxpr/cond/branch_1_fun/reduce_sum | solution.py:31
  144.2 5.6 %fusion.21 = f32[8,256,64]{1,2,0:T(8,128)S(1)} fusion(f32[2048,256,8]{1,0,2:T(8,128)S(1)} %get-tuple-element.412, f32[8,256]{1,0:T(8,128)S(1)} %max.8, f32[8,2048]{1,0:T(8,128)S(1)} %dynamic-slice_bitcast_fusion.2, f32[8,256]{1,0:T(8,128)S(1)} %copy-done.3, pred[256,2048]{0,1:T(8,128)(4,1)S(1)} %broadcast_compare_fusion, ...), kind=kOutput, calls=%fused_computation.21 | convolution fusion | flops 566493184 | bytes 18702336 | tf_op jit(solution)/shard_map/while/body/eval_jaxpr/cond/branch_1_fun/hqk,kd->hqd/dot_general | solution.py:32
  149.9 2.2 fusion.14
  152.0 2.9 fusion.13
  155.0 3.7 %fusion.18 = f32[4,256,128]{2,1,0:T(8,128)S(1)} fusion(f32[2048,256,4]{1,0,2:T(8,128)S(1)} %get-tuple-element.414, f32[4,256]{1,0:T(4,128)S(1)} %max.9, f32[4,2048]{1,0:T(4,128)S(1)} %dynamic-slice_bitcast_fusion.3, f32[4,256]{1,0:T(4,128)S(1)} %copy-done.4, pred[256,2048]{0,1:T(8,128)(4,1)S(1)} %broadcast_compare_fusion, ...), kind=kOutput, calls=%fused_computation.20 | convolution fusion | flops 551813120 | bytes 10530816 | tf_op jit(solution)/shard_map/while/body/eval_jaxpr/cond/branch_1_fun/hqk,kd->hqd/dot_general | solution.py:32
  161.1 0.7 copy.46
  162.4 3.9 %all_to_all.48 = bf16[2,128,512]{2,1,0:T(8,128)(2,1)S(1)} all-to-all(bf16[2,128,512]{2,1,0:T(8,128)(2,1)S(1)} %all_to_all.38), channel_id=1, replica_groups=mesh['sp'=16,'tp'=2] {'tp'}, dimensions={0} | all-to-all | bytes 524288 | tf_op jit(solution)/shard_map/all_to_all | solution.py:160
  166.4 3.4 %all-to-all-start = ((bf16[2,128,512]{1,2,0:T(8,128)(2,1)}), bf16[2,128,512]{1,2,0:T(8,128)(2,1)S(1)}, u32[]{:S(2)}, u32[]{:S(2)}) async-start(bf16[2,128,512]{1,2,0:T(8,128)(2,1)} %copy.46), calls=%async_computation | async-start | bytes 524288 | tf_op jit(solution)/shard_map/all_to_all | solution.py:159
  170.0 1.4 all-to-all-done
  171.4 2.9 fusion.62
  174.3 3.2 multiply_reduce_fusion.1
  177.9 0.8 convolution_convert_fusion
  178.7 78.1 %all_to_all.49 = bf16[32,16,2048]{2,1,0:T(8,128)(2,1)S(1)} all-to-all(bf16[32,16,2048]{2,1,0:T(8,128)(2,1)S(1)} %bitcast.126), channel_id=1, replica_groups=mesh['sp'=16,'tp'=2] {'sp','tp'}, dimensions={0} | all-to-all | bytes 4194304 | tf_op jit(solution)/shard_map/all_to_all | solution.py:181
  256.8 3.7 %fusion.36 = f32[512,1024]{1,0:T(8,128)} fusion(bf16[512,2048]{1,0:T(8,128)(2,1)S(1)} %bitcast.128, bf16[1,2048,1024]{2,1,0:T(8,128)(2,1)S(1)} %copy-done.11), kind=kOutput, calls=%fused_computation.49 | convolution fusion | flops 2147483648 | bytes 8388608 | tf_op jit(solution)/shard_map/dot_general | solution.py:184
  260.5 10.0 %fusion.38 = bf16[512,2048]{1,0:T(8,128)(2,1)} fusion(bf16[1,1024,2048]{2,1,0:T(8,128)(2,1)} %param.35, f32[512,1024]{1,0:T(8,128)} %fusion.36, bf16[512,2048]{1,0:T(8,128)(2,1)S(1)} %bitcast.129, bf16[1,2048,1024]{2,1,0:T(8,128)(2,1)} %param.34), kind=kOutput, calls=%fused_computation.51 | convolution fusion | flops 4299161600 | bytes 14680064 | tf_op jit(solution)/shard_map/dot_general | solution.py:187
  270.4 3.7 %all-to-all-start.3 = ((bf16[32,16,2048]{2,1,0:T(8,128)(2,1)}), bf16[32,16,2048]{2,1,0:T(8,128)(2,1)S(1)}, u32[]{:S(2)}, u32[]{:S(2)}) async-start(bf16[32,16,2048]{2,1,0:T(8,128)(2,1)} %bitcast.127), calls=%async_computation.3 | async-start | bytes 4194304 | tf_op jit(solution)/shard_map/all_to_all | solution.py:188
  274.2 48.6 %all-to-all-done.3 = bf16[32,16,2048]{2,1,0:T(8,128)(2,1)S(1)} async-done(((bf16[32,16,2048]{2,1,0:T(8,128)(2,1)}), bf16[32,16,2048]{2,1,0:T(8,128)(2,1)S(1)}, u32[]{:S(2)}, u32[]{:S(2)}) %all-to-all-start.3) | async-done | bytes 2097184 | tf_op jit(solution)/shard_map/all_to_all | solution.py:188
  322.8 2.3 gather_fusion
  325.2 1.5 convert_element_type.66
  327.0 1.2 fusion.46
  (78 shorter events, 7.6 us)
Async XLA Ops:
  6.5 88.1 %all-gather.3.cloned.1.call-start = ((), (), s32[]{:S(2)}) async-start(), calls=%async_computation.4 | async-start | bytes 1114112 | tf_op jit(solution)/shard_map/all_gather | solution.py:135
  7.3 123.0 %all-gather.5.cloned.1.call-start = ((), (), s32[]{:S(2)}) async-start(), calls=%async_computation.5 | async-start | bytes 2228224 | tf_op jit(solution)/shard_map/all_gather | solution.py:136
  93.1 37.1 %copy-start.6 = (s32[256]{0:T(256)}, s32[256]{0:T(256)S(1)}, u32[]{:S(2)}) copy-start(s32[256]{0:T(256)S(1)} %fusion.58) | copy-start | bytes 3076
  133.0 5.0 %copy-start.3 = (f32[8,256]{1,0:T(8,128)S(1)}, f32[8,256]{1,0:T(8,128)}, u32[]{:S(2)}) copy-start(f32[8,256]{1,0:T(8,128)} %get-tuple-element.221) | copy-start | bytes 24580 | tf_op jit(solution)/shard_map/while/body/eval_jaxpr/cond
  144.1 5.6 %copy-start = (bf16[2,2048,256]{2,1,0:T(8,128)(2,1)S(1)}, bf16[2,2048,256]{2,1,0:T(8,128)(2,1)}, u32[]{:S(2)}) copy-start(bf16[2,2048,256]{2,1,0:T(8,128)(2,1)} %get-tuple-element.226) | copy-start | bytes 6291460 | tf_op jit(solution)/shard_map/while/body/eval_jaxpr/cond
  144.2 5.7 %copy-start.4 = (f32[4,256]{1,0:T(4,128)S(1)}, f32[4,256]{1,0:T(4,128)}, u32[]{:S(2)}) copy-start(f32[4,256]{1,0:T(4,128)} %get-tuple-element.228) | copy-start | bytes 12292 | tf_op jit(solution)/shard_map/while/body/eval_jaxpr/cond
  161.0 16.4 %copy-start.2 = (bf16[128,2048]{1,0:T(8,128)(2,1)S(1)}, bf16[128,2048]{1,0:T(8,128)(2,1)}, u32[]{:S(2)}) copy-start(bf16[128,2048]{1,0:T(8,128)(2,1)} %param.27) | copy-start | bytes 1572868
  161.1 16.4 %copy-start.8 = (f32[2048]{0:T(1024)S(1)}, f32[2048]{0:T(1024)}, u32[]{:S(2)}) copy-start(f32[2048]{0:T(1024)} %param.30) | copy-start | bytes 24580
  162.1 15.8 %copy-start.1 = (bf16[256,512]{1,0:T(8,128)(2,1)S(1)}, bf16[256,512]{1,0:T(8,128)(2,1)}, u32[]{:S(2)}) copy-start(bf16[256,512]{1,0:T(8,128)(2,1)} %fusion.53) | copy-start | bytes 786436
  162.1 15.8 %copy-start.9 = (f32[2048]{0:T(1024)S(1)}, f32[2048]{0:T(1024)}, u32[]{:S(2)}) copy-start(f32[2048]{0:T(1024)} %param.31) | copy-start | bytes 24580
  166.4 5.0 %all-to-all-start = ((bf16[2,128,512]{1,2,0:T(8,128)(2,1)}), bf16[2,128,512]{1,2,0:T(8,128)(2,1)S(1)}, u32[]{:S(2)}, u32[]{:S(2)}) async-start(bf16[2,128,512]{1,2,0:T(8,128)(2,1)} %copy.46), calls=%async_computation | async-start | bytes 524288 | tf_op jit(solution)/shard_map/all_to_all | solution.py:159
  174.3 82.5 %copy-start.11 = (bf16[1,2048,1024]{2,1,0:T(8,128)(2,1)S(1)}, bf16[1,2048,1024]{2,1,0:T(8,128)(2,1)}, u32[]{:S(2)}) copy-start(bf16[1,2048,1024]{2,1,0:T(8,128)(2,1)} %param.33) | copy-start | bytes 12582916
  260.5 13.7 %copy-start.5 = (s32[2,128]{1,0:T(2,128)S(1)}, s32[2,128]{1,0:T(2,128)}, u32[]{:S(2)}) copy-start(s32[2,128]{1,0:T(2,128)} %param.36) | copy-start | bytes 3076
  260.5 13.7 %copy-start.7 = (s32[256]{0:T(256)S(1)}, s32[256]{0:T(256)}, u32[]{:S(2)}) copy-start(s32[256]{0:T(256)} %copy-done.6) | copy-start | bytes 3076
  260.5 13.7 %copy-start.12 = (f32[128]{0:T(128)S(1)}, f32[128]{0:T(128)}, u32[]{:S(2)}) copy-start(f32[128]{0:T(128)} %param.37) | copy-start | bytes 1540
  270.4 52.4 %all-to-all-start.3 = ((bf16[32,16,2048]{2,1,0:T(8,128)(2,1)}), bf16[32,16,2048]{2,1,0:T(8,128)(2,1)S(1)}, u32[]{:S(2)}, u32[]{:S(2)}) async-start(bf16[32,16,2048]{2,1,0:T(8,128)(2,1)} %bitcast.127), calls=%async_computation.3 | async-start | bytes 4194304 | tf_op jit(solution)/shard_map/all_to_all | solution.py:188
  274.1 52.9 %copy-start.10 = (f32[2048]{0:T(1024)S(1)}, f32[2048]{0:T(1024)}, u32[]{:S(2)}) copy-start(f32[2048]{0:T(1024)} %param.32) | copy-start | bytes 24580
Sparse Core Ops, SparseCore 0:
  10.1 58.3 all-gather.2
  71.2 58.9 all-gather.4
where the time goes:
time: 336 us; the launch traced here: 335 us
  blocking collectives  162 us (48%)
  waiting for transfers between devices  85.5 us (25%)
  matrix products  36.9 us (11%)
  other arithmetic  18.1 us (5%)
  between operations  13.7 us (4%)
  local copies, waits for them, and re-layouts  8.6 us (3%)
  starting transfers between devices  7.15 us (2%)
    all_to_all x1, blocking collectives, on_device(): lax.all_to_all(outgoing, ('sp', 'tp'), split_axis=0, concat_axis=0, tiled...  78.1 us
    all_to_all x1, waiting for transfers between devices, on_device(): lax.all_to_all(expert_out.reshape(received.shape), ('sp', 'tp'), split_ax...  48.6 us
    all_gather x1, blocking collectives, on_device(): lax.all_gather(cum_large, 'sp', axis=1, tiled=True)  43.1 us
    all_gather x1, blocking collectives, on_device(): lax.all_gather(cum_small, 'sp', axis=1, tiled=True)  36.7 us
    all_gather x1, waiting for transfers between devices, on_device(): lax.all_gather(kv_large, 'sp', axis=0, tiled=True)  34.1 us
    dot_general x1, matrix products, on_device(): jnp.dot(hidden, w_down[0], preferred_element_type=jnp.float32)  9.97 us
    dot_general x2, matrix products, online_update(): jnp.einsum('hqk,kd->hqd', weights.astype(jnp.bfloat16), value_rows, prefe...  9.26 us
    reduce_sum x2, other arithmetic, online_update(): running_sum = running_sum * factor + jnp.sum(weights, axis=-1)  8.95 us
  transfers between devices with their start and end apart: 4, of which 3 were waited for; matrix products, arithmetic and copies ran while one was open for 3% of the time, Pallas kernels for 0%

commit v1 on v0

--- a/solution.py
+++ b/solution.py
@@ -124,7 +124,7 @@
     query_large = queries_large.reshape(tokens_here, heads_large, size_large)
     query_pos = lax.axis_index("sp") * tokens_here + jnp.arange(tokens_here, dtype=jnp.int32)
     cum_all = (
-        lax.all_gather(cum_small, "sp", axis=1, tiled=True),
+        jnp.concatenate(lax.all_gather(cum_small, "sp"), axis=1),
         lax.all_gather(cum_large, "sp", axis=1, tiled=True),
     )
     start_state = (

time: 336 us -> 336 us (level)
  no operation moved by 1% of the time
where the time goes in v1:
time: 336 us; the launch traced here: 335 us
  blocking collectives  162 us (48%)
  waiting for transfers between devices  85.5 us (25%)
  matrix products  36.9 us (11%)
  other arithmetic  18.1 us (5%)
  between operations  13.7 us (4%)
  local copies, waits for them, and re-layouts  8.6 us (3%)
  starting transfers between devices  7.15 us (2%)
    all_to_all x1, blocking collectives, on_device(): lax.all_to_all(outgoing, ('sp', 'tp'), split_axis=0, concat_axis=0, tiled...  78.1 us
    all_to_all x1, waiting for transfers between devices, on_device(): lax.all_to_all(expert_out.reshape(received.shape), ('sp', 'tp'), split_ax...  48.6 us
    all_gather x1, blocking collectives, on_device(): lax.all_gather(cum_large, 'sp', axis=1, tiled=True)  43.1 us
    all_gather x1, blocking collectives, on_device(): lax.all_gather(cum_small, 'sp')  36.7 us
    all_gather x1, waiting for transfers between devices, on_device(): lax.all_gather(kv_large, 'sp', axis=0, tiled=True)  34.1 us
    dot_general x1, matrix products, on_device(): jnp.dot(hidden, w_down[0], preferred_element_type=jnp.float32)  9.97 us
    dot_general x2, matrix products, online_update(): jnp.einsum('hqk,kd->hqd', weights.astype(jnp.bfloat16), value_rows, prefe...  9.26 us
    reduce_sum x2, other arithmetic, online_update(): running_sum = running_sum * factor + jnp.sum(weights, axis=-1)  8.95 us
  transfers between devices with their start and end apart: 4, of which 3 were waited for; matrix products, arithmetic and copies ran while one was open for 3% of the time, Pallas kernels for 0%

profile of v1, /device:TPU:0, one launch (start us, length us, event | category | flops | bytes accessed | tf_op | source)
XLA Modules:
  0.0 335.0 jit_solution(12341823653482546608)
XLA Ops:
  8.7 1.1 copy.42
  9.8 1.1 copy.43
  12.5 43.1 %all_gather.19 = f32[4,4096]{1,0:T(4,128)S(1)} all-gather(f32[4,256]{1,0:T(4,128)} %param.26), channel_id=1, replica_groups=mesh['sp'=16,'tp'=2] {'sp'}, dimensions={1}, use_global_device_ids=true | all-gather | bytes 69632 | tf_op jit(solution)/shard_map/all_gather | solution.py:128
  55.7 36.7 %all-gather = f32[128,256]{1,0:T(8,128)S(1)} all-gather(f32[8,256]{1,0:T(8,128)} %param.25), channel_id=2, replica_groups=mesh['sp'=16,'tp'=2] {'sp'}, dimensions={0}, use_global_device_ids=true | all-gather | bytes 139264 | tf_op jit(solution)/shard_map/all_gather | solution.py:127
  92.4 0.8 fusion.58
  93.8 0.8 fusion.53
  94.7 1.5 copy.44
  96.2 34.1 %all-gather.6.cloned.1.call-done = bf16[4096,256]{1,0:T(8,128)(2,1)} async-done(((bf16[256,256]{1,0:T(8,128)(2,1)}), bf16[4096,256]{1,0:T(8,128)(2,1)}) %all-gather.6.cloned.1.call-update) | async-done | bytes 2097168 | tf_op jit(solution)/shard_map/all_gather | solution.py:136
  130.4 30.6 %while.21 = (s32[]{:T(128)}, f32[8,256]{1,0:T(8,128)S(1)}, f32[8,256]{1,0:T(8,128)S(1)}, f32[8,256,64]{1,2,0:T(8,128)S(1)}, f32[4,256]{1,0:T(4,128)S(1)}, /*inde...) while((s32[]{:T(128)}, f32[8,256]{1,0:T(8,128)S(1)}, ...), condition=%wide.region_8.9_spmd.clone, body=%wide.region_0.8_spmd.clone.sunk | while | flops 2268078336 | bytes 95699496 | solution.py:81
  130.4 0.7 fusion.72
  132.4 26.2 %conditional.3 = ((f32[8,256]{1,0:T(8,128)S(1)}, f32[8,256]{1,0:T(8,128)S(1)}, f32[8,256,64]{1,2,0:T(8,128)S(1)}, f32[4,256]{1,0:T(4,128)S(1)}, f32[4,256]{1,0:T(4,128)S(1)}, /*index=5*/f32[4,256,128]{2,1,0:T(8,128)S(1)})) conditional(s32[]{:T(128)} %convert_element_type.110, (f32[8,256]{1,0:T(8,128)S(1)}, f32[8,256]{1,0:T(8,128)S(1)}, ...), branch_computations={%region_2.2_spmd, %region_3.7_spmd} | conditional | flops 2268076288 | bytes 95681696 | solution.py:77
  133.0 5.0 %fusion.6 = (f32[8,256]{1,0:T(8,128)S(1)}, f32[2048,256,8]{1,0,2:T(8,128)S(1)}) fusion(f32[8,2048]{1,0:T(8,128)S(1)} %dynamic-slice_bitcast_fusion.2, f32[8,256]{1,0:T(8,128)} %get-tuple-element.221, pred[256,2048]{0,1:T(8,128)(4,1)S(1)} %broadcast_compare_fusion, bf16[256,8,64]{0,2,1:T(8,128)(2,1)S(1)} %get-tuple-element.220, ...), kind=kOutput, calls=%fused_computation.8 | convolution fusion | flops 557840384 | bytes 17907712 | tf_op jit(solution)/shard_map/while/body/eval_jaxpr/cond/branch_1_fun/qhd,kd->hqk/dot_general | solution.py:22
  138.1 6.0 %fusion.5 = f32[8,256]{1,0:T(8,128)S(1)} fusion(f32[2048,256,8]{1,0,2:T(8,128)S(1)} %get-tuple-element.412, f32[8,256]{1,0:T(8,128)S(1)} %max.8, f32[8,2048]{1,0:T(8,128)S(1)} %dynamic-slice_bitcast_fusion.2, f32[8,256]{1,0:T(8,128)S(1)} %copy-done.3, pred[256,2048]{0,1:T(8,128)(4,1)S(1)} %broadcast_compare_fusion), kind=kLoop, calls=%fused_computation.7 | loop fusion | flops 29358080 | bytes 17391616 | tf_op jit(solution)/shard_map/while/body/eval_jaxpr/cond/branch_1_fun/reduce_sum | solution.py:31
  144.2 5.6 %fusion.21 = f32[8,256,64]{1,2,0:T(8,128)S(1)} fusion(f32[2048,256,8]{1,0,2:T(8,128)S(1)} %get-tuple-element.412, f32[8,256]{1,0:T(8,128)S(1)} %max.8, f32[8,2048]{1,0:T(8,128)S(1)} %dynamic-slice_bitcast_fusion.2, f32[8,256]{1,0:T(8,128)S(1)} %copy-done.3, pred[256,2048]{0,1:T(8,128)(4,1)S(1)} %broadcast_compare_fusion, ...), kind=kOutput, calls=%fused_computation.21 | convolution fusion | flops 566493184 | bytes 18702336 | tf_op jit(solution)/shard_map/while/body/eval_jaxpr/cond/branch_1_fun/hqk,kd->hqd/dot_general | solution.py:32
  149.9 2.2 fusion.14
  152.0 2.9 fusion.13
  155.0 3.7 %fusion.18 = f32[4,256,128]{2,1,0:T(8,128)S(1)} fusion(f32[2048,256,4]{1,0,2:T(8,128)S(1)} %get-tuple-element.414, f32[4,256]{1,0:T(4,128)S(1)} %max.9, f32[4,2048]{1,0:T(4,128)S(1)} %dynamic-slice_bitcast_fusion.3, f32[4,256]{1,0:T(4,128)S(1)} %copy-done.4, pred[256,2048]{0,1:T(8,128)(4,1)S(1)} %broadcast_compare_fusion, ...), kind=kOutput, calls=%fused_computation.20 | convolution fusion | flops 551813120 | bytes 10530816 | tf_op jit(solution)/shard_map/while/body/eval_jaxpr/cond/branch_1_fun/hqk,kd->hqd/dot_general | solution.py:32
  161.1 0.7 copy.46
  162.4 3.9 %all_to_all.48 = bf16[2,128,512]{2,1,0:T(8,128)(2,1)S(1)} all-to-all(bf16[2,128,512]{2,1,0:T(8,128)(2,1)S(1)} %all_to_all.38), channel_id=1, replica_groups=mesh['sp'=16,'tp'=2] {'tp'}, dimensions={0} | all-to-all | bytes 524288 | tf_op jit(solution)/shard_map/all_to_all | solution.py:160
  166.4 3.4 %all-to-all-start = ((bf16[2,128,512]{1,2,0:T(8,128)(2,1)}), bf16[2,128,512]{1,2,0:T(8,128)(2,1)S(1)}, u32[]{:S(2)}, u32[]{:S(2)}) async-start(bf16[2,128,512]{1,2,0:T(8,128)(2,1)} %copy.46), calls=%async_computation | async-start | bytes 524288 | tf_op jit(solution)/shard_map/all_to_all | solution.py:159
  170.0 1.4 all-to-all-done
  171.4 2.9 fusion.62
  174.3 3.2 multiply_reduce_fusion.1
  177.9 0.8 convolution_convert_fusion
  178.7 78.1 %all_to_all.49 = bf16[32,16,2048]{2,1,0:T(8,128)(2,1)S(1)} all-to-all(bf16[32,16,2048]{2,1,0:T(8,128)(2,1)S(1)} %bitcast.130), channel_id=1, replica_groups=mesh['sp'=16,'tp'=2] {'sp','tp'}, dimensions={0} | all-to-all | bytes 4194304 | tf_op jit(solution)/shard_map/all_to_all | solution.py:181
  256.8 3.7 %fusion.36 = f32[512,1024]{1,0:T(8,128)} fusion(bf16[512,2048]{1,0:T(8,128)(2,1)S(1)} %bitcast.132, bf16[1,2048,1024]{2,1,0:T(8,128)(2,1)S(1)} %copy-done.11), kind=kOutput, calls=%fused_computation.49 | convolution fusion | flops 2147483648 | bytes 8388608 | tf_op jit(solution)/shard_map/dot_general | solution.py:184
  260.5 10.0 %fusion.38 = bf16[512,2048]{1,0:T(8,128)(2,1)} fusion(bf16[1,1024,2048]{2,1,0:T(8,128)(2,1)} %param.35, f32[512,1024]{1,0:T(8,128)} %fusion.36, bf16[512,2048]{1,0:T(8,128)(2,1)S(1)} %bitcast.133, bf16[1,2048,1024]{2,1,0:T(8,128)(2,1)} %param.34), kind=kOutput, calls=%fused_computation.51 | convolution fusion | flops 4299161600 | bytes 14680064 | tf_op jit(solution)/shard_map/dot_general | solution.py:187
  270.4 3.7 %all-to-all-start.3 = ((bf16[32,16,2048]{2,1,0:T(8,128)(2,1)}), bf16[32,16,2048]{2,1,0:T(8,128)(2,1)S(1)}, u32[]{:S(2)}, u32[]{:S(2)}) async-start(bf16[32,16,2048]{2,1,0:T(8,128)(2,1)} %bitcast.131), calls=%async_computation.3 | async-start | bytes 4194304 | tf_op jit(solution)/shard_map/all_to_all | solution.py:188
  274.2 48.6 %all-to-all-done.3 = bf16[32,16,2048]{2,1,0:T(8,128)(2,1)S(1)} async-done(((bf16[32,16,2048]{2,1,0:T(8,128)(2,1)}), bf16[32,16,2048]{2,1,0:T(8,128)(2,1)S(1)}, u32[]{:S(2)}, u32[]{:S(2)}) %all-to-all-start.3) | async-done | bytes 2097184 | tf_op jit(solution)/shard_map/all_to_all | solution.py:188
  322.8 2.3 gather_fusion
  325.2 1.5 convert_element_type.66
  327.0 1.2 fusion.46
  (78 shorter events, 7.6 us)
Async XLA Ops:
  6.5 88.1 %all-gather.4.cloned.1.call-start = ((), (), s32[]{:S(2)}) async-start(), calls=%async_computation.4 | async-start | bytes 1114112 | tf_op jit(solution)/shard_map/all_gather | solution.py:135
  7.3 123.0 %all-gather.6.cloned.1.call-start = ((), (), s32[]{:S(2)}) async-start(), calls=%async_computation.5 | async-start | bytes 2228224 | tf_op jit(solution)/shard_map/all_gather | solution.py:136
  93.1 37.1 %copy-start.6 = (s32[256]{0:T(256)}, s32[256]{0:T(256)S(1)}, u32[]{:S(2)}) copy-start(s32[256]{0:T(256)S(1)} %fusion.58) | copy-start | bytes 3076
  133.0 5.0 %copy-start.3 = (f32[8,256]{1,0:T(8,128)S(1)}, f32[8,256]{1,0:T(8,128)}, u32[]{:S(2)}) copy-start(f32[8,256]{1,0:T(8,128)} %get-tuple-element.221) | copy-start | bytes 24580 | tf_op jit(solution)/shard_map/while/body/eval_jaxpr/cond
  144.1 5.6 %copy-start = (bf16[2,2048,256]{2,1,0:T(8,128)(2,1)S(1)}, bf16[2,2048,256]{2,1,0:T(8,128)(2,1)}, u32[]{:S(2)}) copy-start(bf16[2,2048,256]{2,1,0:T(8,128)(2,1)} %get-tuple-element.226) | copy-start | bytes 6291460 | tf_op jit(solution)/shard_map/while/body/eval_jaxpr/cond
  144.2 5.7 %copy-start.4 = (f32[4,256]{1,0:T(4,128)S(1)}, f32[4,256]{1,0:T(4,128)}, u32[]{:S(2)}) copy-start(f32[4,256]{1,0:T(4,128)} %get-tuple-element.228) | copy-start | bytes 12292 | tf_op jit(solution)/shard_map/while/body/eval_jaxpr/cond
  161.0 16.4 %copy-start.2 = (bf16[128,2048]{1,0:T(8,128)(2,1)S(1)}, bf16[128,2048]{1,0:T(8,128)(2,1)}, u32[]{:S(2)}) copy-start(bf16[128,2048]{1,0:T(8,128)(2,1)} %param.27) | copy-start | bytes 1572868
  161.1 16.4 %copy-start.8 = (f32[2048]{0:T(1024)S(1)}, f32[2048]{0:T(1024)}, u32[]{:S(2)}) copy-start(f32[2048]{0:T(1024)} %param.30) | copy-start | bytes 24580
  162.1 15.8 %copy-start.1 = (bf16[256,512]{1,0:T(8,128)(2,1)S(1)}, bf16[256,512]{1,0:T(8,128)(2,1)}, u32[]{:S(2)}) copy-start(bf16[256,512]{1,0:T(8,128)(2,1)} %fusion.53) | copy-start | bytes 786436
  162.1 15.8 %copy-start.9 = (f32[2048]{0:T(1024)S(1)}, f32[2048]{0:T(1024)}, u32[]{:S(2)}) copy-start(f32[2048]{0:T(1024)} %param.31) | copy-start | bytes 24580
  166.4 5.0 %all-to-all-start = ((bf16[2,128,512]{1,2,0:T(8,128)(2,1)}), bf16[2,128,512]{1,2,0:T(8,128)(2,1)S(1)}, u32[]{:S(2)}, u32[]{:S(2)}) async-start(bf16[2,128,512]{1,2,0:T(8,128)(2,1)} %copy.46), calls=%async_computation | async-start | bytes 524288 | tf_op jit(solution)/shard_map/all_to_all | solution.py:159
  174.3 82.5 %copy-start.11 = (bf16[1,2048,1024]{2,1,0:T(8,128)(2,1)S(1)}, bf16[1,2048,1024]{2,1,0:T(8,128)(2,1)}, u32[]{:S(2)}) copy-start(bf16[1,2048,1024]{2,1,0:T(8,128)(2,1)} %param.33) | copy-start | bytes 12582916
  260.5 13.7 %copy-start.5 = (s32[2,128]{1,0:T(2,128)S(1)}, s32[2,128]{1,0:T(2,128)}, u32[]{:S(2)}) copy-start(s32[2,128]{1,0:T(2,128)} %param.36) | copy-start | bytes 3076
  260.5 13.7 %copy-start.7 = (s32[256]{0:T(256)S(1)}, s32[256]{0:T(256)}, u32[]{:S(2)}) copy-start(s32[256]{0:T(256)} %copy-done.6) | copy-start | bytes 3076
  260.5 13.7 %copy-start.12 = (f32[128]{0:T(128)S(1)}, f32[128]{0:T(128)}, u32[]{:S(2)}) copy-start(f32[128]{0:T(128)} %param.37) | copy-start | bytes 1540
  270.4 52.4 %all-to-all-start.3 = ((bf16[32,16,2048]{2,1,0:T(8,128)(2,1)}), bf16[32,16,2048]{2,1,0:T(8,128)(2,1)S(1)}, u32[]{:S(2)}, u32[]{:S(2)}) async-start(bf16[32,16,2048]{2,1,0:T(8,128)(2,1)} %bitcast.131), calls=%async_computation.3 | async-start | bytes 4194304 | tf_op jit(solution)/shard_map/all_to_all | solution.py:188
  274.1 52.9 %copy-start.10 = (f32[2048]{0:T(1024)S(1)}, f32[2048]{0:T(1024)}, u32[]{:S(2)}) copy-start(f32[2048]{0:T(1024)} %param.32) | copy-start | bytes 24580
Sparse Core Ops, SparseCore 0:
  10.1 58.3 all-gather.3
  71.2 58.9 all-gather.5
